TPU v7x, 32 devices: a whole 2x2x4 slice. The times are simulated.
32 devices in a mesh: ep: 16 (over z, y, x), tp: 2 (over core).
Axes of the slice: x: 2, y: 2, z: 4, core: 2. Of those that a mesh axis runs over, the one named last changes fastest.
Arguments:
- tokens: bfloat16 [8192, 2048], P(('ep', 'tp')), may hold values from -6 to 6
- norm_gain: float32 [2048], replicated, may hold values from 0.1 to 1.9
- expert_ids: int32 [8192, 2], P(('ep', 'tp')), may hold values from 0 to 15, all different within a row; in each aligned block of 256 rows (0 to 255, 256 to 511, ...) at most 48 rows name the same one
- route_weights: float32 [8192, 2], P(('ep', 'tp')), may hold values from 0.2 to 1.2
- expert_gate: bfloat16 [16, 2048, 512], P('ep', None, 'tp'), may hold values from -0.125 to 0.125
- expert_up: bfloat16 [16, 2048, 512], P('ep', None, 'tp'), may hold values from -0.125 to 0.125
- expert_down: bfloat16 [16, 512, 2048], P('ep', 'tp'), may hold values from -0.25 to 0.25
- shared_gate: bfloat16 [2048, 512], P(None, 'tp'), may hold values from -0.125 to 0.125
- shared_up: bfloat16 [2048, 512], P(None, 'tp'), may hold values from -0.125 to 0.125
- shared_down: bfloat16 [512, 2048], P('tp'), may hold values from -0.25 to 0.25
Outputs:
- mixed: bfloat16 [8192, 2048], P(('ep', 'tp'))
Inputs may be any that keep to these rules, and one draw needn't show every extreme that they name: `expert_ids`: each token names 2 different experts. Among the tokens of one device (aligned blocks of 256 rows) no expert is named by more than 48 tokens, and in every block some expert is named by exactly 48.
All inputs are finite; a program needn't handle non-finite values.
Results may differ from a plain program's by a relative error of at most 0.0075.
Values may be sent and summed in bfloat16 or wider, within the bound.
A program may use at most 64 MiB of HBM per device.

v0:
```python
import jax
import jax.numpy as jnp
from jax import lax
from jax.sharding import PartitionSpec as P

epsilon = 1e-06


def normalize(tokens, norm_gain):
    values = tokens.astype(jnp.float32)
    factor = lax.rsqrt(jnp.mean(values * values, axis=1, keepdims=True) + epsilon)
    return (values * factor * norm_gain[None, :]).astype(jnp.bfloat16)


def round_term(partial_value):
    return lax.optimization_barrier(partial_value.astype(jnp.bfloat16)).astype(jnp.float32)


def gated_rows(row_block, gate_w, up_w):
    gate_value = jnp.dot(row_block, gate_w, preferred_element_type=jnp.float32)
    up_value = jnp.dot(row_block, up_w, preferred_element_type=jnp.float32)
    return (jax.nn.silu(gate_value) * up_value).astype(jnp.bfloat16)


def sliced_term(hidden, down_w):
    return round_term(jnp.dot(hidden, down_w, preferred_element_type=jnp.float32))


def shared_branch(normed, shared_gate, shared_up, shared_down):
    hidden = gated_rows(lax.all_gather(normed, "tp", axis=0, tiled=True), shared_gate, shared_up)
    return lax.psum_scatter(
        sliced_term(hidden, shared_down).astype(jnp.bfloat16), "tp", scatter_dimension=0, tiled=True
    ).astype(jnp.float32)


def body(
    tokens,
    norm_gain,
    expert_ids,
    route_weights,
    expert_gate,
    expert_up,
    expert_down,
    shared_gate,
    shared_up,
    shared_down,
):
    normed = normalize(tokens, norm_gain)
    tok_rows = tokens.shape[0]
    model_width = tokens.shape[1]
    top_count = expert_ids.shape[1]
    ep_size = lax.axis_size("ep")
    experts = expert_gate.shape[0] * ep_size
    capacity = 3 * tok_rows * top_count // (2 * experts)
    assigned = tok_rows * top_count
    gate_one = expert_gate[0]
    up_one = expert_up[0]
    down_one = expert_down[0]
    flat_ids = expert_ids.reshape(-1)
    onehot = (flat_ids[:, None] == jnp.arange(experts, dtype=jnp.int32)[None, :]).astype(
        jnp.bfloat16
    )
    earlier = (jnp.arange(assigned)[:, None] > jnp.arange(assigned)[None, :]).astype(jnp.bfloat16)
    before_count = jnp.dot(earlier, onehot, preferred_element_type=jnp.float32)
    slot_index = jnp.sum(before_count * onehot.astype(jnp.float32), axis=1).astype(jnp.int32)
    position = flat_ids * capacity + slot_index
    owners = (
        jnp.full((experts * capacity,), tok_rows, jnp.int32)
        .at[position]
        .set(jnp.arange(assigned, dtype=jnp.int32) // top_count)
    )
    padded = jnp.concatenate([normed, jnp.zeros((1, model_width), jnp.bfloat16)], axis=0)
    outgoing = padded[owners].reshape(ep_size, capacity, model_width)
    half_slots = capacity // 2
    split_rows = outgoing.reshape(ep_size, 2, half_slots, model_width)
    results = []
    for portion in range(2):
        received = lax.all_to_all(
            split_rows[:, portion], "ep", split_axis=0, concat_axis=0, tiled=True
        )
        hidden = gated_rows(
            lax.all_gather(
                received.reshape(ep_size * half_slots, model_width), "tp", axis=0, tiled=True
            ),
            gate_one,
            up_one,
        )
        summed = lax.psum_scatter(
            sliced_term(hidden, down_one).astype(jnp.bfloat16),
            "tp",
            scatter_dimension=0,
            tiled=True,
        )
        results.append(
            lax.all_to_all(
                summed.reshape(ep_size, half_slots, model_width),
                "ep",
                split_axis=0,
                concat_axis=0,
                tiled=True,
            )
        )
    returned = jnp.stack(results, axis=1)
    gathered = returned.reshape(experts * capacity, model_width)[position]
    routed = jnp.sum(
        gathered.reshape(tok_rows, top_count, model_width).astype(jnp.float32)
        * route_weights[:, :, None],
        axis=1,
    )
    shared_out = shared_branch(normed, shared_gate, shared_up, shared_down)
    return (routed + shared_out).astype(jnp.bfloat16)


def solution(mesh):
    placed = (
        P(("ep", "tp"), None),
        P(),
        P(("ep", "tp"), None),
        P(("ep", "tp"), None),
        P("ep", None, "tp"),
        P("ep", None, "tp"),
        P("ep", "tp", None),
        P(None, "tp"),
        P(None, "tp"),
        P("tp", None),
    )
    return jax.shard_map(
        body, mesh=mesh, in_specs=placed, out_specs=P(("ep", "tp"), None), check_vma=False
    )
```

profile of v0, /device:TPU:12, one launch (start us, length us, event | category | flops | bytes accessed | tf_op | source)
XLA Modules:
  0.0 249.7 jit_solution(8733958691054052228)
XLA Ops:
  6.5 1.0 copy.14
  7.5 0.7 broadcast_multiply_fusion
  8.2 1.5 fusion
  9.7 0.1 eq.15
  9.9 0.3 fusion.6
  10.2 0.1 copy.13
  10.3 0.1 mul.73
  10.5 2.4 scatter_custom_fusion
  12.9 1.0 fusion.2
  14.0 0.1 concatenate.3
  14.1 4.2 %gather_fusion = bf16[768,2048]{1,0:T(8,128)(2,1)} fusion(bf16[257,2048]{1,0:T(8,128)(2,1)S(1)} %concatenate.3, s32[1024]{0:T(1024)S(1)} %pad_clamp_fusion.1), kind=kCustom, calls=%fused_computation | custom fusion | bytes 6294528 | tf_op jit(solution)/shard_map/gather | solution.py:73
  18.3 2.2 slice_bitcast_fusion.1
  20.5 43.5 %all_to_all.20 = bf16[16,24,2048]{2,1,0:T(8,128)(2,1)} all-to-all(bf16[16,24,2048]{2,1,0:T(8,128)(2,1)S(1)} %get-tuple-element.5), channel_id=1, replica_groups=mesh['ep'=16,'tp'=2] {'ep'}, dimensions={0} | all-to-all | bytes 3145728 | tf_op jit(solution)/shard_map/all_to_all | solution.py:78
  64.0 0.0 all-gather.4.cloned.1.call-update
  64.0 0.0 all-gather.6.cloned.1.call-start
  64.1 40.7 %all_to_all.21 = bf16[16,24,2048]{2,1,0:T(8,128)(2,1)} all-to-all(bf16[16,24,2048]{2,1,0:T(8,128)(2,1)S(1)} %get-tuple-element.6), channel_id=1, replica_groups=mesh['ep'=16,'tp'=2] {'ep'}, dimensions={0} | all-to-all | bytes 3145728 | tf_op jit(solution)/shard_map/all_to_all | solution.py:78
  104.8 0.0 all-gather.6.cloned.1.call-update
  104.8 0.0 reduce-scatter.4.cloned.1.call-start
  104.9 0.0 all-gather.4.cloned.1.call-done
  104.9 3.2 %fusion.15 = f32[768,256]{1,0:T(8,128)S(1)} fusion(bf16[768,2048]{1,0:T(8,128)(2,1)} %all-gather.4.cloned.1.call-done, bf16[1,2048,256]{2,1,0:T(8,128)(2,1)} %param.14), kind=kOutput, calls=%fused_computation.30 | convolution fusion | flops 805306368 | bytes 4980736 | tf_op jit(solution)/shard_map/dot_general | solution.py:20
  108.2 6.9 %convolution_convert_fusion.1 = bf16[768,2048]{1,0:T(8,128)(2,1)} fusion(bf16[768,2048]{1,0:T(8,128)(2,1)} %all-gather.4.cloned.1.call-done, bf16[1,256,2048]{2,1,0:T(8,128)(2,1)S(1)} %copy-done, bf16[1,2048,256]{2,1,0:T(8,128)(2,1)S(1)} %copy-done.5, f32[768,256]{1,0:T(8,128)S(1)} %fusion.15), kind=kOutput, calls=%fused_computation.5 | convolution fusion | flops 1613365248 | bytes 9175040 | tf_op jit(solution)/shard_map/dot_general | solution.py:26
  115.0 0.0 reduce-scatter.4.cloned.1.call-update
  115.0 0.0 all-gather.8.cloned.1.call-start
  115.1 0.5 all-gather.8.cloned.1.call-update
  115.6 0.0 reduce-scatter.6.cloned.1.call-start
  115.7 0.8 all-gather.6.cloned.1.call-done
  116.5 3.8 %fusion.13 = f32[768,256]{1,0:T(8,128)} fusion(bf16[768,2048]{1,0:T(8,128)(2,1)} %all-gather.6.cloned.1.call-done, bf16[1,2048,256]{2,1,0:T(8,128)(2,1)S(1)} %copy-done.4), kind=kOutput, calls=%fused_computation.28 | convolution fusion | flops 805306368 | bytes 4980736 | tf_op jit(solution)/shard_map/dot_general | solution.py:20
  120.3 7.1 %convolution_convert_fusion = bf16[768,2048]{1,0:T(8,128)(2,1)} fusion(bf16[768,2048]{1,0:T(8,128)(2,1)} %all-gather.6.cloned.1.call-done, bf16[1,256,2048]{2,1,0:T(8,128)(2,1)S(1)} %copy-done, bf16[1,2048,256]{2,1,0:T(8,128)(2,1)S(1)} %copy-done.5, f32[768,256]{1,0:T(8,128)} %fusion.13), kind=kOutput, calls=%fused_computation.4 | convolution fusion | flops 1613365248 | bytes 9175040 | tf_op jit(solution)/shard_map/dot_general | solution.py:26
  127.4 0.0 reduce-scatter.6.cloned.1.call-update
  127.4 3.8 %reduce-scatter.4.cloned.1.call-done = bf16[384,2048]{1,0:T(8,128)(2,1)} async-done(((bf16[768,2048]{1,0:T(8,128)(2,1)}), bf16[384,2048]{1,0:T(8,128)(2,1)}) %reduce-scatter.4.cloned.1.call-update) | async-done | bytes 1572880 | tf_op jit(solution)/shard_map/reduce_scatter | solution.py:88
  131.2 7.0 %all-to-all-start.1 = ((bf16[16,24,2048]{2,1,0:T(8,128)(2,1)}), bf16[16,24,2048]{2,1,0:T(8,128)(2,1)S(1)}, u32[]{:S(2)}, u32[]{:S(2)}) async-start(bf16[16,24,2048]{2,1,0:T(8,128)(2,1)} %bitcast.45), calls=%async_computation.2 | async-start | bytes 3145728 | tf_op jit(solution)/shard_map/all_to_all | solution.py:95
  138.2 0.2 reduce-scatter.8.cloned.1.call-start
  138.4 6.0 %all-gather.8.cloned.1.call-done = bf16[512,2048]{1,0:T(8,128)(2,1)} async-done(((bf16[256,2048]{1,0:T(8,128)(2,1)}), bf16[512,2048]{1,0:T(8,128)(2,1)}) %all-gather.8.cloned.1.call-update) | async-done | bytes 2097168 | tf_op jit(solution)/shard_map/all_gather | solution.py:30
  144.4 2.6 %fusion.45 = f32[512,256]{1,0:T(8,128)S(1)} fusion(bf16[512,2048]{1,0:T(8,128)(2,1)} %all-gather.8.cloned.1.call-done, bf16[2048,256]{1,0:T(8,128)(2,1)} %param.17), kind=kOutput, calls=%fused_computation.72 | convolution fusion | flops 536870912 | bytes 3670016 | tf_op jit(solution)/shard_map/dot_general | solution.py:20
  147.0 5.8 %convolution_convert_fusion.2 = bf16[512,2048]{1,0:T(8,128)(2,1)} fusion(bf16[256,2048]{1,0:T(8,128)(2,1)} %param.19, bf16[512,2048]{1,0:T(8,128)(2,1)} %all-gather.8.cloned.1.call-done, bf16[2048,256]{1,0:T(8,128)(2,1)} %param.18, f32[512,256]{1,0:T(8,128)S(1)} %fusion.45), kind=kOutput, calls=%fused_computation.7 | convolution fusion | flops 1075576832 | bytes 6815744 | tf_op jit(solution)/shard_map/dot_general | solution.py:26
  152.8 0.0 reduce-scatter.8.cloned.1.call-update
  152.8 6.2 %reduce-scatter.6.cloned.1.call-done = bf16[384,2048]{1,0:T(8,128)(2,1)} async-done(((bf16[768,2048]{1,0:T(8,128)(2,1)}), bf16[384,2048]{1,0:T(8,128)(2,1)}) %reduce-scatter.6.cloned.1.call-update) | async-done | bytes 1572880 | tf_op jit(solution)/shard_map/reduce_scatter | solution.py:88
  158.9 16.5 %all-to-all-done.1 = bf16[16,24,2048]{2,1,0:T(8,128)(2,1)S(1)} async-done(((bf16[16,24,2048]{2,1,0:T(8,128)(2,1)}), bf16[16,24,2048]{2,1,0:T(8,128)(2,1)S(1)}, u32[]{:S(2)}, u32[]{:S(2)}) %all-to-all-start.1) | async-done | bytes 1572896 | tf_op jit(solution)/shard_map/all_to_all | solution.py:95
  175.5 5.0 %all-to-all-start.3 = ((bf16[16,24,2048]{2,1,0:T(8,128)(2,1)}), bf16[16,24,2048]{2,1,0:T(8,128)(2,1)}, u32[]{:S(2)}, u32[]{:S(2)}) async-start(bf16[16,24,2048]{2,1,0:T(8,128)(2,1)} %bitcast.46), calls=%async_computation.5 | async-start | bytes 3145728 | tf_op jit(solution)/shard_map/all_to_all | solution.py:95
  180.5 0.1 copy.16
  180.7 36.4 %all-to-all-done.3 = bf16[16,24,2048]{2,1,0:T(8,128)(2,1)} async-done(((bf16[16,24,2048]{2,1,0:T(8,128)(2,1)}), bf16[16,24,2048]{2,1,0:T(8,128)(2,1)}, u32[]{:S(2)}, u32[]{:S(2)}) %all-to-all-start.3) | async-done | bytes 1572896 | tf_op jit(solution)/shard_map/all_to_all | solution.py:95
  217.1 1.7 pad_maximum_fusion
  218.8 2.1 copy.15
  220.8 6.7 %gather_fusion.1 = bf16[512,2048]{1,0:T(8,128)(2,1)S(1)} fusion(bf16[768,2048]{1,0:T(8,128)(2,1)} %bitcast.40, s32[1024]{0:T(1024)S(1)} %pad_clamp_fusion), kind=kCustom, calls=%fused_computation.1 | custom fusion | bytes 4196352 | tf_op jit(solution)/shard_map/gather | solution.py:104
  227.5 4.0 %reshape.67 = f32[256,2,2048]{2,1,0:T(2,128)} reshape(bf16[512,2048]{1,0:T(8,128)(2,1)S(1)} %gather_fusion.1) | data formatting | bytes 6291456 | tf_op jit(solution)/shard_map/convert_element_type | solution.py:106
  231.5 8.8 %multiply_reduce_fusion = f32[256,2048]{1,0:T(8,128)S(1)} fusion(f32[256,2,2048]{2,1,0:T(2,128)} %reshape.67, f32[256,2]{1,0:T(8,128)S(1)} %copy.16), kind=kLoop, calls=%fused_computation.3 | loop fusion | flops 1572864 | bytes 6293504 | tf_op jit(solution)/shard_map/reduce_sum | solution.py:105
  240.3 0.0 reduce-scatter.8.cloned.1.call-done
  240.4 2.5 add_convert_fusion
  (20 shorter events, 0.1 us)
Async XLA Ops:
  6.5 101.6 %copy-start = (bf16[1,256,2048]{2,1,0:T(8,128)(2,1)S(1)}, bf16[1,256,2048]{2,1,0:T(8,128)(2,1)}, u32[]{:S(2)}) copy-start(bf16[1,256,2048]{2,1,0:T(8,128)(2,1)} %param.16) | copy-start | bytes 3145732
  6.5 6.4 %copy-start.2 = (bf16[256,2048]{1,0:T(8,128)(2,1)S(1)}, bf16[256,2048]{1,0:T(8,128)(2,1)}, u32[]{:S(2)}) copy-start(bf16[256,2048]{1,0:T(8,128)(2,1)} %param.10) | copy-start | bytes 3145732
  6.5 98.4 %all-gather.4.cloned.1.call-start = ((), (), s32[]{:S(2)}) async-start(), calls=%async_computation.7 | async-start | bytes 4718592 | tf_op jit(solution)/shard_map/all_gather | solution.py:82
  14.0 4.4 %copy-start.1 = (bf16[256,2048]{1,0:T(8,128)(2,1)}, bf16[256,2048]{1,0:T(8,128)(2,1)S(1)}, u32[]{:S(2)}) copy-start(bf16[256,2048]{1,0:T(8,128)(2,1)S(1)} %fusion.2) | copy-start | bytes 3145732
  64.0 52.5 %all-gather.6.cloned.1.call-start = ((), (), s32[]{:S(2)}) async-start(), calls=%async_computation.9 | async-start | bytes 4718592 | tf_op jit(solution)/shard_map/all_gather | solution.py:82
  104.8 3.3 %copy-start.5 = (bf16[1,2048,256]{2,1,0:T(8,128)(2,1)S(1)}, bf16[1,2048,256]{2,1,0:T(8,128)(2,1)}, u32[]{:S(2)}) copy-start(bf16[1,2048,256]{2,1,0:T(8,128)(2,1)} %param.15) | copy-start | bytes 3145732
  104.8 26.4 %reduce-scatter.4.cloned.1.call-start = ((), (), s32[]{:S(2)}) async-start(), calls=%async_computation.8 | async-start | bytes 4718592 | tf_op jit(solution)/shard_map/reduce_scatter | solution.py:88
  115.0 1.5 copy-start.4
  115.0 29.3 %all-gather.8.cloned.1.call-start = ((), (), s32[]{:S(2)}) async-start(), calls=%async_computation.11 | async-start | bytes 3145728 | tf_op jit(solution)/shard_map/all_gather | solution.py:30
  115.6 43.3 %reduce-scatter.6.cloned.1.call-start = ((), (), s32[]{:S(2)}) async-start(), calls=%async_computation.10 | async-start | bytes 4718592 | tf_op jit(solution)/shard_map/reduce_scatter | solution.py:88
  131.2 44.3 %all-to-all-start.1 = ((bf16[16,24,2048]{2,1,0:T(8,128)(2,1)}), bf16[16,24,2048]{2,1,0:T(8,128)(2,1)S(1)}, u32[]{:S(2)}, u32[]{:S(2)}) async-start(bf16[16,24,2048]{2,1,0:T(8,128)(2,1)} %bitcast.45), calls=%async_computation.2 | async-start | bytes 3145728 | tf_op jit(solution)/shard_map/all_to_all | solution.py:95
  138.2 102.2 %reduce-scatter.8.cloned.1.call-start = ((), (), s32[]{:S(2)}) async-start(), calls=%async_computation.12 | async-start | bytes 3145728 | tf_op jit(solution)/shard_map/reduce_scatter | solution.py:31
  152.8 27.7 %copy-start.3 = (f32[256,2]{0,1:T(2,128)S(1)}, f32[256,2]{0,1:T(2,128)}, u32[]{:S(2)}) copy-start(f32[256,2]{0,1:T(2,128)} %param.13) | copy-start | bytes 6148
  175.5 41.6 %all-to-all-start.3 = ((bf16[16,24,2048]{2,1,0:T(8,128)(2,1)}), bf16[16,24,2048]{2,1,0:T(8,128)(2,1)}, u32[]{:S(2)}, u32[]{:S(2)}) async-start(bf16[16,24,2048]{2,1,0:T(8,128)(2,1)} %bitcast.46), calls=%async_computation.5 | async-start | bytes 3145728 | tf_op jit(solution)/shard_map/all_to_all | solution.py:95
Sparse Core Ops, SparseCore 0:
  64.1 11.4 all-gather.3
  104.9 11.4 all-gather.5
  118.7 12.4 reduce-scatter.3
  132.6 11.7 all-gather.7
  146.5 12.4 reduce-scatter.5
  161.0 11.0 reduce-scatter.7
where the time goes:
time: 250 us
  blocking collectives  84.2 us (34%)
  waiting for transfers between devices  70.4 us (28%)
  matrix products  29.6 us (12%)
  local copies, waits for them, and re-layouts  23.3 us (9%)
  other arithmetic  16.2 us (6%)
  between operations  13.7 us (5%)
  starting transfers between devices  12.3 us (5%)
    all_to_all x2, blocking collectives, body(): lax.all_to_all(split_rows[:, portion], 'ep', split_axis=0, concat_axis=0,...  84.2 us
    all_to_all x2, waiting for transfers between devices, body(): lax.all_to_all(summed.reshape(ep_size, half_slots, model_width), 'ep', sp...  53 us
    dot_general x3, matrix products, sliced_term(): jnp.dot(hidden, down_w, preferred_element_type=jnp.float32)  19.8 us
    all_to_all x2, starting transfers between devices, body(): lax.all_to_all(summed.reshape(ep_size, half_slots, model_width), 'ep', sp...  12 us
    reduce_scatter x2, waiting for transfers between devices, body(): lax.psum_scatter(sliced_term(hidden, down_one).astype(jnp.bfloat16), 'tp'...  9.96 us
    dot_general x3, matrix products, gated_rows(): gate_value = jnp.dot(row_block, gate_w, preferred_element_type=jnp.float32)  9.57 us
    reduce_sum x1, other arithmetic, body(): jnp.sum(gathered.reshape(tok_rows, top_count, model_width).astype(jnp.flo...  8.79 us
    gather x1, local copies, waits for them, and re-layouts, body(): gathered = returned.reshape(experts * capacity, model_width)[position]  6.7 us
  transfers between devices with their start and end apart: 8, of which 6 were waited for; matrix products, arithmetic and copies ran while one was open for 21% of the time, Pallas kernels for 0%

commit v1 on v0

--- a/solution.py
+++ b/solution.py
@@ -1,9 +1,284 @@
+import functools
+
 import jax
 import jax.numpy as jnp
 from jax import lax
+from jax.experimental import pallas as pl
+from jax.experimental.pallas import tpu as pltpu
 from jax.sharding import PartitionSpec as P
 
 epsilon = 1e-06
+MESH = pl.DeviceIdType.MESH
+
+
+def toggled(index, step, size):
+    total, bit = 0, 1
+    while bit < size:
+        total = total + bit * ((index // bit + step // bit) % 2)
+        bit *= 2
+    return total
+
+
+def gated_sum(rows, gate_w, up_w, down_w):
+    total = None
+    for half in range(gate_w.shape[0]):
+        gate_value = jnp.dot(rows, gate_w[half], preferred_element_type=jnp.float32)
+        up_value = jnp.dot(rows, up_w[half], preferred_element_type=jnp.float32)
+        hidden = (gate_value / (1.0 + jnp.exp(-gate_value)) * up_value).astype(jnp.bfloat16)
+        term = jnp.dot(hidden, down_w[half], preferred_element_type=jnp.float32)
+        total = term if total is None else total + term
+    return total
+
+
+def layer_kernel(
+    peers,
+    capacity,
+    tokens,
+    gain,
+    ids_row,
+    ids_col,
+    weights_col,
+    expert_gate,
+    expert_up,
+    expert_down,
+    shared_gate,
+    shared_up,
+    shared_down,
+    mixed,
+    gate_all,
+    up_all,
+    down_all,
+    s_gate_all,
+    s_up_all,
+    s_down_all,
+    normed,
+    outgoing,
+    received,
+    results,
+    returned,
+    total,
+    weight_local,
+    weight_send,
+    weight_recv,
+    out_send,
+    out_recv,
+    back_send,
+    back_recv,
+):
+    me = lax.axis_index("ep")
+    core = lax.axis_index("tp")
+    sibling = 1 - core
+    tok_rows = tokens.shape[0]
+    group = 4
+    barrier = pltpu.get_barrier_semaphore()
+    pl.semaphore_signal(barrier, inc=1, device_id=(me, sibling), device_id_type=MESH)
+    for step in range(1, peers):
+        pl.semaphore_signal(
+            barrier, inc=1, device_id=(toggled(me, step, peers), core), device_id_type=MESH
+        )
+    sources = (
+        (shared_gate, s_gate_all),
+        (shared_up, s_up_all),
+        (shared_down, s_down_all),
+        (expert_gate, gate_all),
+        (expert_up, up_all),
+        (expert_down, down_all),
+    )
+    local = [
+        pltpu.make_async_copy(source, target.at[core], weight_local.at[i])
+        for i, (source, target) in enumerate(sources)
+    ]
+    for copy in local:
+        copy.start()
+
+    values = tokens[...].astype(jnp.float32)
+    factor = lax.rsqrt(jnp.mean(values * values, axis=1, keepdims=True) + epsilon)
+    normed[...] = (values * factor * gain[...]).astype(jnp.bfloat16)
+
+    relative = ids_row[...] ^ me
+    step_of = lax.broadcasted_iota(jnp.int32, (peers, tok_rows), 0)
+    named = (step_of == relative[0:1, :]) | (step_of == relative[1:2, :])
+    row_at = lax.broadcasted_iota(jnp.int32, (tok_rows, tok_rows), 0)
+    col_at = lax.broadcasted_iota(jnp.int32, (tok_rows, tok_rows), 1)
+    before = jnp.where(row_at < col_at, 1.0, 0.0).astype(jnp.bfloat16)
+    slots = jnp.dot(
+        jnp.where(named, 1.0, 0.0).astype(jnp.bfloat16), before, preferred_element_type=jnp.float32
+    ).astype(jnp.int32)
+    slots = jnp.where(named, slots, -1)
+    slot_at = lax.broadcasted_iota(jnp.int32, (capacity, tok_rows), 0)
+
+    def pick(step):
+        return jnp.where(slot_at == slots[step : step + 1, :], 1.0, 0.0).astype(jnp.bfloat16)
+
+    def dispatch(step):
+        return pltpu.make_async_remote_copy(
+            src_ref=outgoing.at[step],
+            dst_ref=received.at[step],
+            send_sem=out_send.at[step],
+            recv_sem=out_recv.at[step],
+            device_id=(toggled(me, step, peers), core),
+            device_id_type=MESH,
+        )
+
+    def give_back(step):
+        return pltpu.make_async_remote_copy(
+            src_ref=results.at[step],
+            dst_ref=returned.at[step],
+            send_sem=back_send.at[step],
+            recv_sem=back_recv.at[step],
+            device_id=(toggled(me, step, peers), core),
+            device_id_type=MESH,
+        )
+
+    started = False
+    for first in range(peers - group, -1, -group):
+        picked = jnp.concatenate([pick(first + i) for i in range(group)], axis=0)
+        rows = jnp.dot(picked, normed[...], preferred_element_type=jnp.float32).astype(jnp.bfloat16)
+        for i in range(group):
+            block = rows[i * capacity : (i + 1) * capacity]
+            if first + i == 0:
+                received[0] = block
+            else:
+                outgoing[first + i] = block
+        if not started:
+            pl.semaphore_wait(barrier, peers)
+            started = True
+        for i in range(group):
+            if first + i:
+                dispatch(first + i).start()
+
+    remote = [
+        pltpu.make_async_remote_copy(
+            src_ref=source,
+            dst_ref=target.at[core],
+            send_sem=weight_send.at[i],
+            recv_sem=weight_recv.at[i],
+            device_id=(me, sibling),
+            device_id_type=MESH,
+        )
+        for i, (source, target) in enumerate(sources)
+    ]
+    for copy in remote:
+        copy.start()
+    for i in range(len(sources)):
+        local[i].wait()
+        remote[i].wait()
+
+    def take(pair, carry):
+        for i in range(2):
+            step = 2 * pair + i
+
+            @pl.when(step > 0)
+            def _():
+                dispatch(step).wait_recv()
+
+        block = received[pl.ds(2 * pair, 2)].reshape(2 * capacity, received.shape[2])
+        out = gated_sum(block, gate_all, up_all, down_all).astype(jnp.bfloat16)
+        for i in range(2):
+            step = 2 * pair + i
+            part = out[i * capacity : (i + 1) * capacity]
+
+            @pl.when(step > 0)
+            def _():
+                results[step] = part
+                give_back(step).start()
+
+            @pl.when(step == 0)
+            def _():
+                returned[step] = part
+
+        return carry
+
+    total[...] = gated_sum(normed[...], s_gate_all, s_up_all, s_down_all)
+    lax.fori_loop(0, peers // 2, take, 0)
+
+    relative_col = ids_col[...] ^ me
+    expert_at = lax.broadcasted_iota(jnp.int32, (tok_rows, 128), 1)
+    chosen = [expert_at == relative_col[:, j : j + 1] for j in range(2)]
+    after = jnp.where(row_at > col_at, 1.0, 0.0).astype(jnp.bfloat16)
+    counted = jnp.dot(
+        after,
+        jnp.where(chosen[0] | chosen[1], 1.0, 0.0).astype(jnp.bfloat16),
+        preferred_element_type=jnp.float32,
+    )
+    places = [
+        relative_col[:, j : j + 1] * capacity
+        + jnp.sum(jnp.where(chosen[j], counted, 0.0), axis=1, keepdims=True).astype(jnp.int32)
+        for j in range(2)
+    ]
+    for first in range(0, peers, group):
+        for i in range(group):
+            if first + i:
+                give_back(first + i).wait_recv()
+        at = lax.broadcasted_iota(jnp.int32, (tok_rows, group * capacity), 1) + first * capacity
+        scale = jnp.where(at == places[0], weights_col[:, 0:1], 0.0) + jnp.where(
+            at == places[1], weights_col[:, 1:2], 0.0
+        )
+        upper = scale.astype(jnp.bfloat16)
+        lower = (scale - upper.astype(jnp.float32)).astype(jnp.bfloat16)
+        block = returned[first : first + group].reshape(group * capacity, returned.shape[2])
+        term = jnp.dot(upper, block, preferred_element_type=jnp.float32) + jnp.dot(
+            lower, block, preferred_element_type=jnp.float32
+        )
+        if first + group < peers:
+            total[...] += term
+        else:
+            mixed[...] = (total[...] + term).astype(jnp.bfloat16)
+    for step in range(1, peers):
+        dispatch(step).wait_send()
+        give_back(step).wait_send()
+
+
+def kernel_body(
+    tokens,
+    norm_gain,
+    expert_ids,
+    route_weights,
+    expert_gate,
+    expert_up,
+    expert_down,
+    shared_gate,
+    shared_up,
+    shared_down,
+):
+    peers = lax.axis_size("ep")
+    halves = lax.axis_size("tp")
+    tok_rows, width = tokens.shape
+    capacity = 3 * tok_rows * expert_ids.shape[1] // (2 * peers)
+    vmem = pl.BlockSpec(memory_space=pltpu.VMEM)
+    anywhere = pl.BlockSpec(memory_space=pl.ANY)
+    slots = pltpu.VMEM((peers, capacity, width), jnp.bfloat16)
+    weights = (
+        expert_gate[0],
+        expert_up[0],
+        expert_down[0],
+        shared_gate,
+        shared_up,
+        shared_down,
+    )
+    dma = pltpu.SemaphoreType.DMA
+    return pl.pallas_call(
+        functools.partial(layer_kernel, peers, capacity),
+        out_shape=jax.ShapeDtypeStruct((tok_rows, width), jnp.bfloat16),
+        in_specs=[vmem] * 5 + [anywhere] * 6,
+        out_specs=vmem,
+        scratch_shapes=[pltpu.VMEM((halves,) + w.shape, w.dtype) for w in weights]
+        + [pltpu.VMEM((tok_rows, width), jnp.bfloat16), slots, slots, slots, slots]
+        + [pltpu.VMEM((tok_rows, width), jnp.float32)]
+        + [dma((len(weights),))] * 3
+        + [dma((peers,))] * 4,
+        compiler_params=pltpu.CompilerParams(
+            collective_id=0, has_side_effects=True, vmem_limit_bytes=56 * 1024 * 1024
+        ),
+        name="layer",
+    )(
+        tokens,
+        norm_gain.reshape(1, width),
+        expert_ids.T,
+        expert_ids,
+        route_weights,
+        *weights,
+    )
 
 
 def normalize(tokens, norm_gain):
@@ -111,6 +386,14 @@
     return (routed + shared_out).astype(jnp.bfloat16)
 
 
+def plan_of(*args):
+    peers = lax.axis_size("ep")
+    capacity = 3 * args[0].shape[0] * args[2].shape[1] // (2 * peers)
+    whole_tiles = capacity % 16 == 0 and peers % 4 == 0 and peers & (peers - 1) == 0
+    fits = whole_tiles and lax.axis_size("tp") == 2 and args[4].shape[0] == 1
+    return (kernel_body if fits else body)(*args)
+
+
 def solution(mesh):
     placed = (
         P(("ep", "tp"), None),
@@ -125,5 +408,5 @@
         P("tp", None),
     )
     return jax.shard_map(
-        body, mesh=mesh, in_specs=placed, out_specs=P(("ep", "tp"), None), check_vma=False
-    )
+        plan_of, mesh=mesh, in_specs=placed, out_specs=P(("ep", "tp"), None), check_vma=False
+    )

time: 250 us -> 160 us (0.64)
  Pallas kernels: 0 us -> 153 us
  blocking collectives: 84.2 us -> 0 us
  waiting for transfers between devices: 70.4 us -> 0 us
  matrix products: 29.6 us -> 0 us
  local copies, waits for them, and re-layouts: 23.3 us -> 4.58 us
  other arithmetic: 16.2 us -> 0 us
  between operations: 13.7 us -> 0.01 us
  starting transfers between devices: 12.3 us -> 0 us
    pallas_call x0 -> x1, Pallas kernels: none -> 153 us  [kernel_body(): pl.pallas_call(functools.partial(layer_kernel, peers, capacity), out_shap...]
    all_to_all x2 -> x0, blocking collectives: 84.2 us -> none  [body(): lax.all_to_all(split_rows[:, portion], 'ep', split_axis=0, concat_axis=0,...]
    all_to_all x2 -> x0, waiting for transfers between devices: 53 us -> none  [body(): lax.all_to_all(summed.reshape(ep_size, half_slots, model_width), 'ep', sp...]
    dot_general x7 -> x0, matrix products: 29.6 us -> none  [the longest x3 19.8 us: sliced_term(): jnp.dot(hidden, down_w, preferred_element_type=jnp.float32)]
    all_to_all x2 -> x0, starting transfers between devices: 12 us -> none  [body(): lax.all_to_all(summed.reshape(ep_size, half_slots, model_width), 'ep', sp...]
    gather x2 -> x0, local copies, waits for them, and re-layouts: 10.9 us -> none  [the longest x1 6.7 us: body(): gathered = returned.reshape(experts * capacity, model_width)[position]]
    reduce_sum x2 -> x0, other arithmetic: 10.3 us -> none  [the longest x1 8.79 us: body(): jnp.sum(gathered.reshape(tok_rows, top_count, model_width).astype(jnp.flo...]
    reduce_scatter x3 -> x0, waiting for transfers between devices: 9.98 us -> none  [the longest x2 9.96 us: body(): lax.psum_scatter(sliced_term(hidden, down_one).astype(jnp.bfloat16), 'tp'...]
  transfers between devices with their start and end apart: 8 -> 0, of which waited for: 6 -> 0; matrix products, arithmetic and copies ran while one was open for 21% -> 0% of each run, Pallas kernels for 0% -> 0%
where the time goes in v1:
time: 160 us; the launch traced here: 158 us
  Pallas kernels  153 us (96%)
  local copies, waits for them, and re-layouts  4.58 us (3%)
    pallas_call x1, Pallas kernels, kernel_body(): pl.pallas_call(functools.partial(layer_kernel, peers, capacity), out_shap...  153 us
    unnamed x7, local copies, waits for them, and re-layouts  4.58 us

profile of v1, /device:TPU:12, one launch (start us, length us, event | category | flops | bytes accessed | tf_op | source)
XLA Modules:
  0.0 157.6 jit_solution(4451077729537119471)
XLA Ops:
  0.0 0.0 copy-start.1
  0.0 0.7 copy-done.1
  0.7 0.0 copy-start
  0.7 0.8 copy.12.weights_col
  1.5 0.0 copy-done
  1.5 0.8 copy.11.ids_col
  2.3 153.0 %layer.1 = bf16[256,2048]{1,0:T(8,128)(2,1)} custom-call(bf16[256,2048]{1,0:T(8,128)(2,1)} %tokens.1, f32[1,2048]{1,0:T(1,128)} %bitcast.8, s32[2,256]{1,0:T(2,128)} %bitcast.9, s32[256,2]{1,0:T(8,128)} %copy.11.ids_col, f32[256,2]{1,0:T(8,128)} %copy.12.weights_col, bf16[2048,256]{1,0:T(8,128)(2,1)} %bitcast.5, bf16[2048,256]{1,0:T(8,128)(2,1)} %bitcast.6, ...), custom_call_target="tpu_custom_call" | custom-call | tf_op jit(solution)/shard_map/layer/pallas_call | solution.py:260
  155.3 2.3 %copy.14 = bf16[256,2048]{1,0:T(8,128)(2,1)} copy(bf16[256,2048]{1,0:T(8,128)(2,1)} %layer.1) | data formatting | bytes 2097152
Async XLA Ops:
  0.0 0.7 copy-start.1
  0.7 0.8 copy-start

commit v2 on v1

--- a/solution.py
+++ b/solution.py
@@ -30,14 +30,75 @@
     return total
 
 
+def slot_rows(meta, me, steps):
+    count = meta.shape[1]
+    relative = meta[0:2, :].astype(jnp.int32) ^ me
+    step_of = lax.broadcasted_iota(jnp.int32, (steps, count), 0)
+    named = (step_of == relative[0:1, :]) | (step_of == relative[1:2, :])
+    row_at = lax.broadcasted_iota(jnp.int32, (count, count), 0)
+    col_at = lax.broadcasted_iota(jnp.int32, (count, count), 1)
+    before = jnp.where(row_at < col_at, 1.0, 0.0).astype(jnp.bfloat16)
+    slots = jnp.dot(
+        jnp.where(named, 1.0, 0.0).astype(jnp.bfloat16), before, preferred_element_type=jnp.float32
+    ).astype(jnp.int32)
+    return jnp.where(named, slots, -1)
+
+
+def picks(slots, steps, capacity):
+    slot_at = lax.broadcasted_iota(jnp.int32, (capacity, slots.shape[1]), 0)
+    return jnp.concatenate(
+        [
+            jnp.where(slot_at == slots[step : step + 1, :], 1.0, 0.0).astype(jnp.bfloat16)
+            for step in steps
+        ],
+        axis=0,
+    )
+
+
+def slot_places(meta, me, capacity):
+    count = meta.shape[1]
+    turned = jnp.transpose(meta)
+    relative = turned[:, 0:2].astype(jnp.int32) ^ me
+    expert_at = lax.broadcasted_iota(jnp.int32, (count, 128), 1)
+    row_at = lax.broadcasted_iota(jnp.int32, (count, count), 0)
+    col_at = lax.broadcasted_iota(jnp.int32, (count, count), 1)
+    chosen = [expert_at == relative[:, j : j + 1] for j in range(2)]
+    after = jnp.where(row_at > col_at, 1.0, 0.0).astype(jnp.bfloat16)
+    counted = jnp.dot(
+        after,
+        jnp.where(chosen[0] | chosen[1], 1.0, 0.0).astype(jnp.bfloat16),
+        preferred_element_type=jnp.float32,
+    )
+    places = [
+        relative[:, j : j + 1] * capacity
+        + jnp.sum(jnp.where(chosen[j], counted, 0.0), axis=1, keepdims=True).astype(jnp.int32)
+        for j in range(2)
+    ]
+    return places, [turned[:, 2 + j : 3 + j] for j in range(2)]
+
+
+def weight_matrix(places, weights, first, amount):
+    at = lax.broadcasted_iota(jnp.int32, (places[0].shape[0], amount), 1) + first
+    scale = jnp.where(at == places[0], weights[0], 0.0) + jnp.where(
+        at == places[1], weights[1], 0.0
+    )
+    upper = scale.astype(jnp.bfloat16)
+    return upper, (scale - upper.astype(jnp.float32)).astype(jnp.bfloat16)
+
+
+def weighted(pair, block):
+    return jnp.dot(pair[0], block, preferred_element_type=jnp.float32) + jnp.dot(
+        pair[1], block, preferred_element_type=jnp.float32
+    )
+
+
 def layer_kernel(
     peers,
     capacity,
+    pieces,
     tokens,
     gain,
-    ids_row,
-    ids_col,
-    weights_col,
+    meta,
     expert_gate,
     expert_up,
     expert_down,
@@ -52,11 +113,18 @@
     s_up_all,
     s_down_all,
     normed,
+    cut,
     outgoing,
     received,
     results,
     returned,
     total,
+    relay_in,
+    meta_in,
+    relay_out,
+    relay_back,
+    sums_out,
+    sums_in,
     weight_local,
     weight_send,
     weight_recv,
@@ -64,18 +132,48 @@
     out_recv,
     back_send,
     back_recv,
+    block_send,
+    block_recv,
+    meta_send,
+    meta_recv,
+    relay_send,
+    relay_recv,
+    home_send,
+    home_recv,
+    sums_send,
+    sums_recv,
 ):
     me = lax.axis_index("ep")
     core = lax.axis_index("tp")
     sibling = 1 - core
-    tok_rows = tokens.shape[0]
-    group = 4
+    width = tokens.shape[1]
+    piece = width // pieces
+    half, quarter = peers // 2, peers // 4
+
+    def is_inner(index):
+        return ((index // quarter + 1) // 2) % 2
+
+    inner = is_inner(me)
+    turns = (half, half + quarter)
+
+    def at_step(step):
+        return (toggled(me, step, peers), core)
+
+    def remote(source, target, send, recv, place):
+        return pltpu.make_async_remote_copy(
+            src_ref=source,
+            dst_ref=target,
+            send_sem=send,
+            recv_sem=recv,
+            device_id=place,
+            device_id_type=MESH,
+        )
+
     barrier = pltpu.get_barrier_semaphore()
+    partners = list(range(1, half)) + list(turns)
     pl.semaphore_signal(barrier, inc=1, device_id=(me, sibling), device_id_type=MESH)
-    for step in range(1, peers):
-        pl.semaphore_signal(
-            barrier, inc=1, device_id=(toggled(me, step, peers), core), device_id_type=MESH
-        )
+    for step in partners:
+        pl.semaphore_signal(barrier, inc=1, device_id=at_step(step), device_id_type=MESH)
     sources = (
         (shared_gate, s_gate_all),
         (shared_up, s_up_all),
@@ -93,78 +191,117 @@
 
     values = tokens[...].astype(jnp.float32)
     factor = lax.rsqrt(jnp.mean(values * values, axis=1, keepdims=True) + epsilon)
-    normed[...] = (values * factor * gain[...]).astype(jnp.bfloat16)
-
-    relative = ids_row[...] ^ me
-    step_of = lax.broadcasted_iota(jnp.int32, (peers, tok_rows), 0)
-    named = (step_of == relative[0:1, :]) | (step_of == relative[1:2, :])
-    row_at = lax.broadcasted_iota(jnp.int32, (tok_rows, tok_rows), 0)
-    col_at = lax.broadcasted_iota(jnp.int32, (tok_rows, tok_rows), 1)
-    before = jnp.where(row_at < col_at, 1.0, 0.0).astype(jnp.bfloat16)
-    slots = jnp.dot(
-        jnp.where(named, 1.0, 0.0).astype(jnp.bfloat16), before, preferred_element_type=jnp.float32
-    ).astype(jnp.int32)
-    slots = jnp.where(named, slots, -1)
-    slot_at = lax.broadcasted_iota(jnp.int32, (capacity, tok_rows), 0)
-
-    def pick(step):
-        return jnp.where(slot_at == slots[step : step + 1, :], 1.0, 0.0).astype(jnp.bfloat16)
+    scaled = (values * factor * gain[...]).astype(jnp.bfloat16)
+    normed[...] = scaled
+    for c in range(pieces):
+        cut[c] = scaled[:, c * piece : (c + 1) * piece]
+
+    gateway = at_step(half + quarter * inner)
+
+    def block_copy(c):
+        return remote(
+            cut.at[c], relay_in.at[inner, c], block_send.at[c], block_recv.at[inner, c], gateway
+        )
+
+    meta_copy = remote(meta, meta_in.at[inner], meta_send.at[0], meta_recv.at[inner], gateway)
+
+    def send_block():
+        meta_copy.start()
+        for c in range(pieces):
+            block_copy(c).start()
 
     def dispatch(step):
-        return pltpu.make_async_remote_copy(
-            src_ref=outgoing.at[step],
-            dst_ref=received.at[step],
-            send_sem=out_send.at[step],
-            recv_sem=out_recv.at[step],
-            device_id=(toggled(me, step, peers), core),
-            device_id_type=MESH,
+        return remote(
+            outgoing.at[step],
+            received.at[step],
+            out_send.at[step],
+            out_recv.at[step],
+            at_step(step),
         )
 
     def give_back(step):
-        return pltpu.make_async_remote_copy(
-            src_ref=results.at[step],
-            dst_ref=returned.at[step],
-            send_sem=back_send.at[step],
-            recv_sem=back_recv.at[step],
-            device_id=(toggled(me, step, peers), core),
-            device_id_type=MESH,
-        )
-
-    started = False
-    for first in range(peers - group, -1, -group):
-        picked = jnp.concatenate([pick(first + i) for i in range(group)], axis=0)
-        rows = jnp.dot(picked, normed[...], preferred_element_type=jnp.float32).astype(jnp.bfloat16)
-        for i in range(group):
+        return remote(
+            results.at[step],
+            returned.at[step],
+            back_send.at[step],
+            back_recv.at[step],
+            at_step(step),
+        )
+
+    pl.semaphore_wait(barrier, len(partners) + 1)
+
+    @pl.when(inner == 1)
+    def _():
+        send_block()
+
+    slots = slot_rows(meta[...], me, half)
+    for first in (quarter, 0):
+        rows = jnp.dot(
+            picks(slots, range(first, first + quarter), capacity),
+            normed[...],
+            preferred_element_type=jnp.float32,
+        ).astype(jnp.bfloat16)
+        for i in range(quarter):
             block = rows[i * capacity : (i + 1) * capacity]
             if first + i == 0:
                 received[0] = block
             else:
                 outgoing[first + i] = block
-        if not started:
-            pl.semaphore_wait(barrier, peers)
-            started = True
-        for i in range(group):
-            if first + i:
                 dispatch(first + i).start()
 
-    remote = [
-        pltpu.make_async_remote_copy(
-            src_ref=source,
-            dst_ref=target.at[core],
-            send_sem=weight_send.at[i],
-            recv_sem=weight_recv.at[i],
-            device_id=(me, sibling),
-            device_id_type=MESH,
-        )
+    @pl.when(inner == 0)
+    def _():
+        send_block()
+
+    swaps = [
+        remote(source, target.at[core], weight_send.at[i], weight_recv.at[i], (me, sibling))
         for i, (source, target) in enumerate(sources)
     ]
-    for copy in remote:
+    for copy in swaps:
         copy.start()
+
+    def relay(side, k, c):
+        turn = turns[side]
+        columns = pl.ds(c * piece, piece)
+        return remote(
+            relay_out.at[side, k, :, columns],
+            received.at[k ^ turn, :, columns],
+            relay_send.at[side * half + k, c],
+            relay_recv.at[(k ^ turn) - half, c],
+            at_step(k),
+        )
+
+    def pass_on(side):
+        remote(
+            meta, meta_in.at[side], meta_send.at[0], meta_recv.at[side], at_step(turns[side])
+        ).wait_recv()
+        picked = picks(slot_rows(meta_in[side], me, half), range(half), capacity)
+        for c in range(pieces):
+            columns = pl.ds(c * piece, piece)
+            remote(
+                cut.at[c],
+                relay_in.at[side, c],
+                block_send.at[c],
+                block_recv.at[side, c],
+                at_step(turns[side]),
+            ).wait_recv()
+            rows = jnp.dot(
+                picked, relay_in[side, c], preferred_element_type=jnp.float32
+            ).astype(jnp.bfloat16)
+            received[turns[side], :, columns] = rows[:capacity]
+            for k in range(half - 1, 0, -1):
+                relay_out[side, k, :, columns] = rows[k * capacity : (k + 1) * capacity]
+                relay(side, k, c).start()
+
+    @pl.when(inner == 1)
+    def _():
+        pass_on(1)
+
     for i in range(len(sources)):
         local[i].wait()
-        remote[i].wait()
-
-    def take(pair, carry):
+        swaps[i].wait()
+
+    def near(pair, carry):
         for i in range(2):
             step = 2 * pair + i
 
@@ -172,7 +309,7 @@
             def _():
                 dispatch(step).wait_recv()
 
-        block = received[pl.ds(2 * pair, 2)].reshape(2 * capacity, received.shape[2])
+        block = received[pl.ds(2 * pair, 2)].reshape(2 * capacity, width)
         out = gated_sum(block, gate_all, up_all, down_all).astype(jnp.bfloat16)
         for i in range(2):
             step = 2 * pair + i
@@ -190,43 +327,133 @@
         return carry
 
     total[...] = gated_sum(normed[...], s_gate_all, s_up_all, s_down_all)
-    lax.fori_loop(0, peers // 2, take, 0)
-
-    relative_col = ids_col[...] ^ me
-    expert_at = lax.broadcasted_iota(jnp.int32, (tok_rows, 128), 1)
-    chosen = [expert_at == relative_col[:, j : j + 1] for j in range(2)]
-    after = jnp.where(row_at > col_at, 1.0, 0.0).astype(jnp.bfloat16)
-    counted = jnp.dot(
-        after,
-        jnp.where(chosen[0] | chosen[1], 1.0, 0.0).astype(jnp.bfloat16),
-        preferred_element_type=jnp.float32,
-    )
-    places = [
-        relative_col[:, j : j + 1] * capacity
-        + jnp.sum(jnp.where(chosen[j], counted, 0.0), axis=1, keepdims=True).astype(jnp.int32)
-        for j in range(2)
-    ]
-    for first in range(0, peers, group):
-        for i in range(group):
-            if first + i:
-                give_back(first + i).wait_recv()
-        at = lax.broadcasted_iota(jnp.int32, (tok_rows, group * capacity), 1) + first * capacity
-        scale = jnp.where(at == places[0], weights_col[:, 0:1], 0.0) + jnp.where(
-            at == places[1], weights_col[:, 1:2], 0.0
-        )
-        upper = scale.astype(jnp.bfloat16)
-        lower = (scale - upper.astype(jnp.float32)).astype(jnp.bfloat16)
-        block = returned[first : first + group].reshape(group * capacity, returned.shape[2])
-        term = jnp.dot(upper, block, preferred_element_type=jnp.float32) + jnp.dot(
-            lower, block, preferred_element_type=jnp.float32
-        )
-        if first + group < peers:
-            total[...] += term
-        else:
-            mixed[...] = (total[...] + term).astype(jnp.bfloat16)
-    for step in range(1, peers):
+    lax.fori_loop(0, half // 2, near, 0)
+
+    @pl.when(inner == 1)
+    def _():
+        pass_on(0)
+
+    def side_of(step):
+        side = is_inner(toggled(me, step, peers))
+        return side, toggled(step, half + quarter * side, peers)
+
+    def home(step):
+        side, k = side_of(step)
+        return remote(
+            results.at[step],
+            relay_back.at[side, k],
+            home_send.at[step - half],
+            home_recv.at[side * half + k],
+            at_step(k),
+        )
+
+    def far(pair, carry):
+        start = half + (2 * pair + quarter * inner) % half
+        for i in range(2):
+            step = start + i
+            side, k = side_of(step)
+
+            @pl.when(k > 0)
+            def _():
+                for c in range(pieces):
+                    columns = pl.ds(c * piece, piece)
+                    remote(
+                        relay_out.at[0, 1, :, columns],
+                        received.at[step, :, columns],
+                        relay_send.at[1, c],
+                        relay_recv.at[step - half, c],
+                        at_step(1),
+                    ).wait_recv()
+
+        block = received[pl.ds(start, 2)].reshape(2 * capacity, width)
+        out = gated_sum(block, gate_all, up_all, down_all).astype(jnp.bfloat16)
+        for i in range(2):
+            step = start + i
+            side, k = side_of(step)
+            part = out[i * capacity : (i + 1) * capacity]
+
+            @pl.when(k > 0)
+            def _():
+                results[step] = part
+                home(step).start()
+
+            @pl.when(k == 0)
+            def _():
+                relay_back[side, 0] = part
+
+        return carry
+
+    lax.fori_loop(0, half // 2, far, 0)
+
+    def sums(side, c):
+        return remote(
+            sums_out.at[side, c],
+            sums_in.at[c],
+            sums_send.at[side * pieces + c],
+            sums_recv.at[c],
+            at_step(turns[side]),
+        )
+
+    @pl.when(inner == 1)
+    def _():
+        for side in (1, 0):
+            places, scales = slot_places(meta_in[side], me, capacity)
+            pair = weight_matrix(places, scales, 0, half * capacity)
+            for k in range(1, half):
+                remote(
+                    results.at[half],
+                    relay_back.at[side, k],
+                    home_send.at[0],
+                    home_recv.at[side * half + k],
+                    at_step(k),
+                ).wait_recv()
+            for c in range(pieces):
+                block = relay_back[side, :, :, pl.ds(c * piece, piece)]
+                sums_out[side, c] = weighted(
+                    pair, block.reshape(half * capacity, piece)
+                ).astype(jnp.bfloat16)
+                sums(side, c).start()
+
+    places, scales = slot_places(meta[...], me, capacity)
+    for step in range(1, half):
+        give_back(step).wait_recv()
+    pair = weight_matrix(places, scales, 0, half * capacity)
+    total[...] += weighted(pair, returned[...].reshape(half * capacity, width))
+    for c in range(pieces):
+        remote(
+            sums_out.at[0, c], sums_in.at[c], sums_send.at[c], sums_recv.at[c], gateway
+        ).wait_recv()
+        columns = pl.ds(c * piece, piece)
+        mixed[:, columns] = (total[:, columns] + sums_in[c].astype(jnp.float32)).astype(
+            jnp.bfloat16
+        )
+
+    for step in range(1, half):
         dispatch(step).wait_send()
         give_back(step).wait_send()
+    meta_copy.wait_send()
+    for c in range(pieces):
+        block_copy(c).wait_send()
+
+    def settle(i, carry):
+        step = half + i
+        _, k = side_of(step)
+
+        @pl.when(k > 0)
+        def _():
+            home(step).wait_send()
+
+        return carry
+
+    lax.fori_loop(0, half, settle, 0)
+
+    @pl.when(inner == 1)
+    def _():
+        for side in range(2):
+            for c in range(pieces):
+                sums(side, c).wait_send()
+                for k in range(1, half):
+                    relay(side, k, c).wait_send()
 
 
 def kernel_body(
@@ -245,9 +472,9 @@
     halves = lax.axis_size("tp")
     tok_rows, width = tokens.shape
     capacity = 3 * tok_rows * expert_ids.shape[1] // (2 * peers)
+    half, pieces = peers // 2, 4
     vmem = pl.BlockSpec(memory_space=pltpu.VMEM)
     anywhere = pl.BlockSpec(memory_space=pl.ANY)
-    slots = pltpu.VMEM((peers, capacity, width), jnp.bfloat16)
     weights = (
         expert_gate[0],
         expert_up[0],
@@ -256,29 +483,47 @@
         shared_up,
         shared_down,
     )
+    meta = jnp.concatenate(
+        [expert_ids.astype(jnp.float32), route_weights, jnp.zeros((tok_rows, 4), jnp.float32)],
+        axis=1,
+    ).T
+
+    def rows(*shape):
+        return pltpu.VMEM(shape, jnp.bfloat16)
+
     dma = pltpu.SemaphoreType.DMA
     return pl.pallas_call(
-        functools.partial(layer_kernel, peers, capacity),
+        functools.partial(layer_kernel, peers, capacity, pieces),
         out_shape=jax.ShapeDtypeStruct((tok_rows, width), jnp.bfloat16),
-        in_specs=[vmem] * 5 + [anywhere] * 6,
+        in_specs=[vmem] * 3 + [anywhere] * 6,
         out_specs=vmem,
         scratch_shapes=[pltpu.VMEM((halves,) + w.shape, w.dtype) for w in weights]
-        + [pltpu.VMEM((tok_rows, width), jnp.bfloat16), slots, slots, slots, slots]
-        + [pltpu.VMEM((tok_rows, width), jnp.float32)]
+        + [
+            rows(tok_rows, width),
+            rows(pieces, tok_rows, width // pieces),
+            rows(half, capacity, width),
+            rows(peers, capacity, width),
+            rows(peers, capacity, width),
+            rows(half, capacity, width),
+            pltpu.VMEM((tok_rows, width), jnp.float32),
+            rows(2, pieces, tok_rows, width // pieces),
+            pltpu.VMEM((2,) + meta.shape, jnp.float32),
+            rows(2, half, capacity, width),
+            rows(2, half, capacity, width),
+            rows(2, pieces, tok_rows, width // pieces),
+            rows(pieces, tok_rows, width // pieces),
+        ]
         + [dma((len(weights),))] * 3
-        + [dma((peers,))] * 4,
+        + [dma((half,))] * 4
+        + [dma((pieces,)), dma((2, pieces)), dma((1,)), dma((2,))]
+        + [dma((2 * half, pieces)), dma((half, pieces))]
+        + [dma((half,)), dma((2 * half,))]
+        + [dma((2 * pieces,)), dma((pieces,))],
         compiler_params=pltpu.CompilerParams(
-            collective_id=0, has_side_effects=True, vmem_limit_bytes=56 * 1024 * 1024
+            collective_id=0, has_side_effects=True, vmem_limit_bytes=60 * 1024 * 1024
         ),
         name="layer",
-    )(
-        tokens,
-        norm_gain.reshape(1, width),
-        expert_ids.T,
-        expert_ids,
-        route_weights,
-        *weights,
-    )
+    )(tokens, norm_gain.reshape(1, width), meta, *weights)
 
 
 def normalize(tokens, norm_gain):

time: 160 us -> 158 us (0.988)
  the two profiles are of different devices: /device:TPU:12 before, /device:TPU:0 now
where the time goes in v2:
time: 158 us
  Pallas kernels  154 us (97%)
  local copies, waits for them, and re-layouts  3.66 us (2%)
    pallas_call x1, Pallas kernels, kernel_body(): pl.pallas_call(functools.partial(layer_kernel, peers, capacity, pieces),...  154 us
    unnamed x5, local copies, waits for them, and re-layouts  3.58 us

profile of v2, /device:TPU:0, one launch (start us, length us, event | category | flops | bytes accessed | tf_op | source)
XLA Modules:
  0.0 158.2 jit_solution(12032058985251426213)
XLA Ops:
  0.0 0.0 copy-start.1
  0.0 0.1 pad.2.clone
  0.1 0.6 copy-done.1
  0.7 0.0 copy-start
  0.7 0.7 copy-done
  1.4 0.7 maximum_bitcast_fusion.meta
  2.0 153.9 %layer.1 = bf16[256,2048]{1,0:T(8,128)(2,1)} custom-call(bf16[256,2048]{1,0:T(8,128)(2,1)} %tokens.1, f32[1,2048]{1,0:T(1,128)} %bitcast.9, f32[8,256]{1,0:T(8,128)} %maximum_bitcast_fusion.meta, bf16[2048,256]{1,0:T(8,128)(2,1)} %bitcast.6, bf16[2048,256]{1,0:T(8,128)(2,1)} %bitcast.7, bf16[256,2048]{1,0:T(8,128)(2,1)} %bitcast.8, ...), custom_call_target="tpu_custom_call" | custom-call | tf_op jit(solution)/shard_map/layer/pallas_call | solution.py:495
  155.9 2.3 %copy.12 = bf16[256,2048]{1,0:T(8,128)(2,1)} copy(bf16[256,2048]{1,0:T(8,128)(2,1)} %layer.1) | data formatting | bytes 2097152
  (2 shorter events, 0.0 us)
Async XLA Ops:
  0.0 0.7 copy-start.1
  0.7 0.7 copy-start

commit v3 on v2

--- a/solution.py
+++ b/solution.py
@@ -170,7 +170,7 @@
         )
 
     barrier = pltpu.get_barrier_semaphore()
-    partners = list(range(1, half)) + list(turns)
+    partners = range(1, peers)
     pl.semaphore_signal(barrier, inc=1, device_id=(me, sibling), device_id_type=MESH)
     for step in partners:
         pl.semaphore_signal(barrier, inc=1, device_id=at_step(step), device_id_type=MESH)
@@ -234,8 +234,9 @@
     def _():
         send_block()
 
-    slots = slot_rows(meta[...], me, half)
-    for first in (quarter, 0):
+    slots = slot_rows(meta[...], me, peers)
+
+    def send_slots(first):
         rows = jnp.dot(
             picks(slots, range(first, first + quarter), capacity),
             normed[...],
@@ -249,9 +250,13 @@
                 outgoing[first + i] = block
                 dispatch(first + i).start()
 
+    send_slots(quarter)
+    send_slots(0)
+
     @pl.when(inner == 0)
     def _():
-        send_block()
+        send_slots(half + quarter)
+        send_slots(half)
 
     swaps = [
         remote(source, target.at[core], weight_send.at[i], weight_recv.at[i], (me, sibling))
@@ -329,10 +334,6 @@
     total[...] = gated_sum(normed[...], s_gate_all, s_up_all, s_down_all)
     lax.fori_loop(0, half // 2, near, 0)
 
-    @pl.when(inner == 1)
-    def _():
-        pass_on(0)
-
     def side_of(step):
         side = is_inner(toggled(me, step, peers))
         return side, toggled(step, half + quarter * side, peers)
@@ -353,7 +354,11 @@
             step = start + i
             side, k = side_of(step)
 
-            @pl.when(k > 0)
+            @pl.when(side == 0)
+            def _():
+                dispatch(step).wait_recv()
+
+            @pl.when((side == 1) & (k > 0))
             def _():
                 for c in range(pieces):
                     columns = pl.ds(c * piece, piece)
@@ -372,14 +377,19 @@
             side, k = side_of(step)
             part = out[i * capacity : (i + 1) * capacity]
 
-            @pl.when(k > 0)
+            @pl.when(side == 0)
+            def _():
+                results[step] = part
+                give_back(step).start()
+
+            @pl.when((side == 1) & (k > 0))
             def _():
                 results[step] = part
                 home(step).start()
 
-            @pl.when(k == 0)
-            def _():
-                relay_back[side, 0] = part
+            @pl.when((side == 1) & (k == 0))
+            def _():
+                relay_back[1, 0] = part
 
         return carry
 
@@ -396,7 +406,7 @@
 
     @pl.when(inner == 1)
     def _():
-        for side in (1, 0):
+        for side in (1,):
             places, scales = slot_places(meta_in[side], me, capacity)
             pair = weight_matrix(places, scales, 0, half * capacity)
             for k in range(1, half):
@@ -418,28 +428,45 @@
     for step in range(1, half):
         give_back(step).wait_recv()
     pair = weight_matrix(places, scales, 0, half * capacity)
-    total[...] += weighted(pair, returned[...].reshape(half * capacity, width))
-    for c in range(pieces):
-        remote(
-            sums_out.at[0, c], sums_in.at[c], sums_send.at[c], sums_recv.at[c], gateway
-        ).wait_recv()
-        columns = pl.ds(c * piece, piece)
-        mixed[:, columns] = (total[:, columns] + sums_in[c].astype(jnp.float32)).astype(
-            jnp.bfloat16
-        )
+    total[...] += weighted(pair, returned[:half].reshape(half * capacity, width))
+
+    @pl.when(inner == 1)
+    def _():
+        for c in range(pieces):
+            sums(1, c).wait_recv()
+            columns = pl.ds(c * piece, piece)
+            mixed[:, columns] = (total[:, columns] + sums_in[c].astype(jnp.float32)).astype(
+                jnp.bfloat16
+            )
+
+    @pl.when(inner == 0)
+    def _():
+        for first in (half, half + quarter):
+            for i in range(quarter):
+                give_back(first + i).wait_recv()
+            pair = weight_matrix(places, scales, first * capacity, quarter * capacity)
+            block = returned[first : first + quarter].reshape(quarter * capacity, width)
+            term = total[...] + weighted(pair, block)
+            if first == half:
+                total[...] = term
+            else:
+                mixed[...] = term.astype(jnp.bfloat16)
+        for step in range(half, peers):
+            dispatch(step).wait_send()
 
     for step in range(1, half):
         dispatch(step).wait_send()
         give_back(step).wait_send()
-    meta_copy.wait_send()
-    for c in range(pieces):
-        block_copy(c).wait_send()
 
     def settle(i, carry):
         step = half + i
-        _, k = side_of(step)
-
-        @pl.when(k > 0)
+        side, k = side_of(step)
+
+        @pl.when(side == 0)
+        def _():
+            give_back(step).wait_send()
+
+        @pl.when((side == 1) & (k > 0))
         def _():
             home(step).wait_send()
 
@@ -449,8 +476,10 @@
 
     @pl.when(inner == 1)
     def _():
-        for side in range(2):
+        meta_copy.wait_send()
+        for side in (1,):
             for c in range(pieces):
+                block_copy(c).wait_send()
                 sums(side, c).wait_send()
                 for k in range(1, half):
                     relay(side, k, c).wait_send()
@@ -501,10 +530,10 @@
         + [
             rows(tok_rows, width),
             rows(pieces, tok_rows, width // pieces),
-            rows(half, capacity, width),
             rows(peers, capacity, width),
             rows(peers, capacity, width),
-            rows(half, capacity, width),
+            rows(peers, capacity, width),
+            rows(peers, capacity, width),
             pltpu.VMEM((tok_rows, width), jnp.float32),
             rows(2, pieces, tok_rows, width // pieces),
             pltpu.VMEM((2,) + meta.shape, jnp.float32),
@@ -514,7 +543,7 @@
             rows(pieces, tok_rows, width // pieces),
         ]
         + [dma((len(weights),))] * 3
-        + [dma((half,))] * 4
+        + [dma((peers,))] * 4
         + [dma((pieces,)), dma((2, pieces)), dma((1,)), dma((2,))]
         + [dma((2 * half, pieces)), dma((half, pieces))]
         + [dma((half,)), dma((2 * half,))]

time: 158 us -> 143 us (0.905)
  the two profiles are of different devices: /device:TPU:0 before, /device:TPU:12 now
where the time goes in v3:
time: 143 us; the launch traced here: 141 us
  Pallas kernels  137 us (96%)
  local copies, waits for them, and re-layouts  3.66 us (3%)
    pallas_call x1, Pallas kernels, kernel_body(): pl.pallas_call(functools.partial(layer_kernel, peers, capacity, pieces),...  137 us
    unnamed x5, local copies, waits for them, and re-layouts  3.58 us

profile of v3, /device:TPU:12, one launch (start us, length us, event | category | flops | bytes accessed | tf_op | source)
XLA Modules:
  0.0 141.1 jit_solution(14975725850406835986)
XLA Ops:
  0.0 0.0 copy-start.1
  0.0 0.1 pad.2.clone
  0.1 0.6 copy-done.1
  0.7 0.0 copy-start
  0.7 0.7 copy-done
  1.4 0.7 maximum_bitcast_fusion.meta
  2.0 136.7 %layer.1 = bf16[256,2048]{1,0:T(8,128)(2,1)} custom-call(bf16[256,2048]{1,0:T(8,128)(2,1)} %tokens.1, f32[1,2048]{1,0:T(1,128)} %bitcast.9, f32[8,256]{1,0:T(8,128)} %maximum_bitcast_fusion.meta, bf16[2048,256]{1,0:T(8,128)(2,1)} %bitcast.6, bf16[2048,256]{1,0:T(8,128)(2,1)} %bitcast.7, bf16[256,2048]{1,0:T(8,128)(2,1)} %bitcast.8, ...), custom_call_target="tpu_custom_call" | custom-call | tf_op jit(solution)/shard_map/layer/pallas_call | solution.py:524
  138.8 2.3 %copy.12 = bf16[256,2048]{1,0:T(8,128)(2,1)} copy(bf16[256,2048]{1,0:T(8,128)(2,1)} %layer.1) | data formatting | bytes 2097152
  (2 shorter events, 0.0 us)
Async XLA Ops:
  0.0 0.7 copy-start.1
  0.7 0.7 copy-start
